TPU v7x, 256 devices: a whole 4x4x8 slice. The times are simulated.
256 devices in a mesh: sp: 64 (over z, x, core), tp: 4 (over y).
Axes of the slice: x: 4, y: 4, z: 8, core: 2. Of those that a mesh axis runs over, the one named last changes fastest.
Arguments:
- queries: bfloat16 [32768, 2048], P('sp', 'tp'), may hold values from -90 to 90, as said below
- key_rows: bfloat16 [32768, 512], P('sp', 'tp'), may hold values from -6 to 6
- value_rows: bfloat16 [32768, 512], P('sp', 'tp'), may hold values from -6 to 6
- sink_logits: float32 [16], P('tp'), may hold values from 2 to 7
- residual: bfloat16 [32768, 2048], P('sp'), may hold values from -6 to 6
- norm_gain: float32 [2048], replicated, may hold values from 0.1 to 1.9
- out_weight: bfloat16 [2048, 2048], P('tp'), may hold values from -1.5 to 1.5
- gate_weight: bfloat16 [2048, 5632], P('sp', 'tp'), may hold values from -0.125 to 0.125
- up_weight: bfloat16 [2048, 5632], P('sp', 'tp'), may hold values from -0.125 to 0.125
- down_weight: bfloat16 [5632, 2048], P('tp', 'sp'), may hold values from -0.078125 to 0.078125
Outputs:
- mixed: bfloat16 [32768, 2048], P(('sp', 'tp'))
Inputs may be any that keep to these rules, and one draw needn't show every extreme that they name: queries are mostly of order one; some rows may be much larger.
All inputs are finite; a program needn't handle non-finite values.
Results may differ from a plain program's by a relative error of at most 0.012.
Values may be sent and summed in bfloat16 or wider, within the bound.
A program may use at most 128 MiB of HBM per device.

v0:
```python
import jax
import jax.numpy as jnp
from jax import lax
from jax.sharding import PartitionSpec as P

DH = 128
WIN = 128
EPSILON = 1e-06
MASKED = -1e30


def with_halo(cells, sides, width):
    for axis, dim in sides:
        count = lax.axis_size(axis)
        ends = count - 1
        head = lax.slice_in_dim(cells, 0, width, axis=dim)
        tail = lax.slice_in_dim(cells, cells.shape[dim] - width, cells.shape[dim], axis=dim)
        cells = jnp.concatenate(
            [
                lax.ppermute(tail, axis, [(i, (i + 1) % count) for i in range(ends)]),
                cells,
                lax.ppermute(head, axis, [((i + 1) % count, i) for i in range(ends)]),
            ],
            axis=dim,
        )
    return cells


def split_up(value, dim, size):
    before, after = (value.shape[:dim], value.shape[dim + 1 :])
    return jnp.moveaxis(value.reshape(*before, size, -1, *after), dim, 0)


def sent_and_summed(value, axis, dim):
    size = lax.axis_size(axis)
    blocks = lax.all_to_all(split_up(value, dim, size), axis, 0, 0, tiled=True)
    return jnp.sum(blocks.astype(jnp.float32), axis=0)


def sent_to_all(value, axis):
    size = lax.axis_size(axis)
    return lax.all_to_all(
        jnp.broadcast_to(value[None], (size, *value.shape)), axis, 0, 0, tiled=True
    )


def laid_out(blocks, dim):
    blocks = jnp.moveaxis(blocks, 0, dim)
    lengths = blocks.shape
    return blocks.reshape(*lengths[:dim], lengths[dim] * lengths[dim + 1], *lengths[dim + 2 :])


def gather_directly(value, axis, dim):
    blocks = sent_to_all(value, axis)
    return laid_out(blocks, dim)


def side_by_side(arrays, axis, dim, along):
    ends, at = ([], 0)
    for a in arrays[:-1]:
        at += a.shape[along]
        ends.append(at)
    both = jnp.concatenate(arrays, axis=along)
    return tuple(jnp.split(lax.all_gather(both, axis, axis=dim, tiled=True), ends, axis=along))


def attend_block(query_blk, key_blk, value_blk, sink_logits, query_pos, key_pos, seq_len):
    kv_heads = key_blk.shape[1] // DH
    group_size = query_blk.shape[1] // key_blk.shape[1]
    query_four = query_blk.reshape(query_blk.shape[0], kv_heads, group_size, DH)
    key_three = key_blk.reshape(key_blk.shape[0], kv_heads, DH)
    value_three = value_blk.reshape(value_blk.shape[0], kv_heads, DH)
    scores = jnp.einsum(
        "qhgd,khd->hgqk", query_four, key_three, preferred_element_type=jnp.float32
    ) * DH ** (-0.5)
    allowed = (
        (jnp.abs(key_pos[None, :] - query_pos[:, None]) <= WIN)
        & (key_pos[None, :] >= 0)
        & (key_pos[None, :] < seq_len)
    )
    scores = jnp.where(allowed[None, None], scores, MASKED)
    sink_col = sink_logits.reshape(kv_heads, group_size)[:, :, None]
    highest = jnp.maximum(jnp.max(scores, axis=-1), sink_col)
    weights_exp = jnp.exp(scores - highest[..., None])
    denominator = jnp.sum(weights_exp, axis=-1) + jnp.exp(sink_col - highest)
    probabilities = (weights_exp / denominator[..., None]).astype(jnp.bfloat16)
    heads_out = jnp.einsum(
        "hgqk,khd->qhgd", probabilities, value_three, preferred_element_type=jnp.float32
    )
    return heads_out.astype(jnp.bfloat16).reshape(query_blk.shape[0], kv_heads * group_size * DH)


def rms_scale(rows_wide, norm_gain):
    mean_square = jnp.mean(rows_wide * rows_wide, axis=-1, keepdims=True)
    return (rows_wide * lax.rsqrt(mean_square + EPSILON) * norm_gain).astype(jnp.bfloat16)


def fetch_down(down_weight):
    return lax.all_gather(down_weight, "sp", axis=1, tiled=True)


def shards(
    queries,
    key_rows,
    value_rows,
    sink_logits,
    residual,
    norm_gain,
    out_weight,
    gate_weight,
    up_weight,
    down_weight,
):
    tok_local = queries.shape[0]
    block_len = 2 * WIN
    share_rows = tok_local // lax.axis_size("tp")
    seq_len = tok_local * lax.axis_size("sp")
    device_offset = lax.axis_index("sp") * tok_local
    kv_pair = jnp.stack([key_rows, value_rows])
    kv_ext = with_halo(kv_pair, (("sp", 1),), WIN)

    def one_block(block_index):
        block_first = block_index * block_len
        query_blk = lax.dynamic_slice_in_dim(queries, block_first, block_len, 0)
        key_blk = lax.dynamic_slice_in_dim(kv_ext[0], block_first, block_len + 2 * WIN, 0)
        value_blk = lax.dynamic_slice_in_dim(kv_ext[1], block_first, block_len + 2 * WIN, 0)
        query_pos = device_offset + block_first + jnp.arange(block_len, dtype=jnp.int32)
        key_pos = (
            device_offset + block_first - WIN + jnp.arange(block_len + 2 * WIN, dtype=jnp.int32)
        )
        return attend_block(query_blk, key_blk, value_blk, sink_logits, query_pos, key_pos, seq_len)

    blocks = lax.map(one_block, jnp.arange(tok_local // block_len, dtype=jnp.int32))
    attended = blocks.reshape(tok_local, queries.shape[1])
    own_first = lax.axis_index("tp") * share_rows
    picked = attended
    attn_share = sent_and_summed(
        jnp.dot(picked, out_weight, preferred_element_type=jnp.float32).astype(jnp.bfloat16),
        "tp",
        0,
    )
    middle_own = (
        lax.dynamic_slice_in_dim(residual, own_first, share_rows, 0).astype(jnp.float32)
        + attn_share
    )
    normed_all = gather_directly(rms_scale(middle_own, norm_gain), "tp", 0)
    pieces = side_by_side((gate_weight, up_weight), "sp", 0, 1)
    gate_sectioned = pieces[0]
    up_sectioned = pieces[1]
    gate_acc = jnp.dot(normed_all, gate_sectioned, preferred_element_type=jnp.float32)
    up_acc = jnp.dot(normed_all, up_sectioned, preferred_element_type=jnp.float32)
    down_whole = fetch_down(down_weight)
    hidden = (jax.nn.silu(gate_acc) * up_acc).astype(jnp.bfloat16)
    picked = hidden
    ffn_share = lax.psum_scatter(
        jnp.dot(picked, down_whole, preferred_element_type=jnp.float32).astype(jnp.bfloat16),
        "tp",
        scatter_dimension=0,
        tiled=True,
    ).astype(jnp.float32)
    return (middle_own + ffn_share).astype(jnp.bfloat16)


def solution(mesh):
    placed = (
        P("sp", "tp"),
        P("sp", "tp"),
        P("sp", "tp"),
        P("tp"),
        P("sp", None),
        P(),
        P("tp", None),
        P("sp", "tp"),
        P("sp", "tp"),
        P("tp", "sp"),
    )
    return jax.shard_map(
        shards, mesh=mesh, in_specs=placed, out_specs=P(("sp", "tp"), None), check_vma=False
    )
```

profile of v0, /device:TPU:1, one launch (start us, length us, event | category | flops | bytes accessed | tf_op | source)
XLA Modules:
  0.0 233.1 jit_solution(577112236005821725)
XLA Ops:
  6.5 1.8 pad_maximum_fusion.1
  8.4 0.7 all-gather.5.cloned.1.call-update
  9.1 0.8 pad_maximum_fusion.3
  9.9 4.5 %collective-permute-start = (bf16[2,128,128]{2,1,0:T(8,128)(2,1)S(1)}, bf16[2,128,128]{2,1,0:T(8,128)(2,1)S(1)}, u32[]{:S(2)}, u32[]{:S(2)}) collective-permute-start(bf16[2,128,128]{2,1,0:T(8,128)(2,1)S(1)} %get-tuple-element.122), channel_id=1, source_target_pairs={{0,4},{4,8},{8,12},{12,16},{16,20},{20,24},{24,28},{28,32},{32,36}... | collective-permute-start | bytes 196616 | tf_op jit(solution)/shard_map/ppermute | solution.py:20
  14.4 1.9 collective-permute-start.1
  16.4 3.6 %collective-permute-done.1 = bf16[2,128,128]{2,1,0:T(8,128)(2,1)S(1)} collective-permute-done((bf16[2,128,128]{2,1,0:T(8,128)(2,1)S(1)}, bf16[2,128,128]{2,1,0:T(8,128)(2,1)S(1)}, u32[]{:S(2)}, u32[]{:S(2)}) %collective-permute-start.1) | collective-permute-done | bytes 65568 | tf_op jit(solution)/shard_map/ppermute | solution.py:22
  20.0 1.0 pad_maximum_fusion
  21.0 11.1 %while.12 = (s32[]{:T(128)}, bf16[2,256,512]{2,1,0:T(8,128)(2,1)}, bf16[2,768,128]{2,1,0:T(8,128)(2,1)S(1)}, s32[2]{0:T(128)S(1)}, s32[]{:T(128)}, /*index=5*/bf...) while((s32[]{:T(128)}, bf16[2,256,512]{2,1,0:T(8,128)(2,1)}, ...), condition=%wide.region_3.4_spmd, body=%wide.region_0.3_spmd.sunk | while | flops 273420544 | bytes 14467520 | solution.py:133
  21.0 0.6 dynamic_slice.48
  22.6 1.0 constant_dynamic-slice_fusion.2
  23.7 0.5 fusion.47
  24.3 0.3 fusion.48
  24.7 0.5 convolution_convert_fusion.4
  25.4 0.4 copy-done.4
  25.8 0.8 copy-done.5
  26.6 0.6 dynamic_slice.48
  28.1 1.0 constant_dynamic-slice_fusion.2
  29.3 0.5 fusion.47
  30.2 0.5 convolution_convert_fusion.4
  30.9 0.4 copy-done.4
  31.3 0.8 copy-done.5
  32.1 3.6 %convolution_convert_fusion.1 = bf16[512,2048]{1,0:T(8,128)(2,1)} fusion(bf16[512,512]{1,0:T(8,128)(2,1)} %bitcast.59, bf16[512,2048]{1,0:T(8,128)(2,1)S(1)} %copy-done), kind=kOutput, calls=%fused_computation.30 | convolution fusion | flops 1074790400 | bytes 4718592 | tf_op jit(solution)/shard_map/dot_general | solution.py:138
  35.7 4.4 %all-to-all-start = ((bf16[4,128,2048]{2,1,0:T(8,128)(2,1)}), bf16[4,128,2048]{2,1,0:T(8,128)(2,1)}, u32[]{:S(2)}, u32[]{:S(2)}) async-start(bf16[4,128,2048]{2,1,0:T(8,128)(2,1)} %bitcast.52), calls=%async_computation | async-start | bytes 4194304 | tf_op jit(solution)/shard_map/all_to_all | solution.py:36
  40.2 24.7 %all-to-all-done = bf16[4,128,2048]{2,1,0:T(8,128)(2,1)} async-done(((bf16[4,128,2048]{2,1,0:T(8,128)(2,1)}), bf16[4,128,2048]{2,1,0:T(8,128)(2,1)}, u32[]{:S(2)}, u32[]{:S(2)}) %all-to-all-start) | async-done | bytes 2097184 | tf_op jit(solution)/shard_map/all_to_all | solution.py:36
  64.9 2.2 convert_reduce_fusion
  67.9 30.0 %all_to_all.10 = bf16[4,128,2048]{2,1,0:T(8,128)(2,1)} all-to-all(bf16[4,128,2048]{2,1,0:T(8,128)(2,1)S(1)} %broadcast_in_dim.44), channel_id=1, replica_groups=mesh['sp'=64,'tp'=4] {'tp'}, dimensions={0} | all-to-all | bytes 4194304 | tf_op jit(solution)/shard_map/all_to_all | solution.py:42
  97.9 4.1 %all-gather.3.cloned.1.call-done = bf16[2048,2816]{1,0:T(8,128)(2,1)} async-done(((bf16[32,2816]{1,0:T(8,128)(2,1)}), bf16[2048,2816]{1,0:T(8,128)(2,1)}) %all-gather.3.cloned.1.call-update) | async-done | bytes 11534352 | tf_op jit(solution)/shard_map/all_gather | solution.py:64
  102.0 8.2 %fusion.14 = f32[512,1408]{1,0:T(8,128)} fusion(bf16[512,2048]{1,0:T(8,128)(2,1)} %bitcast.53, bf16[2048,2816]{1,0:T(8,128)(2,1)} %all-gather.3.cloned.1.call-done), kind=kOutput, calls=%fused_computation.25 | convolution fusion | flops 2952790016 | bytes 10747904 | tf_op jit(solution)/shard_map/dot_general | solution.py:150
  110.2 71.3 %all-gather.5.cloned.1.call-done = bf16[1408,2048]{0,1:T(8,128)(2,1)} async-done(((bf16[1408,32]{0,1:T(8,128)(2,1)}), bf16[1408,2048]{0,1:T(8,128)(2,1)}) %all-gather.5.cloned.1.call-update) | async-done | bytes 5767184 | tf_op jit(solution)/shard_map/all_gather | solution.py:99
  181.5 13.8 %convolution_convert_fusion.2 = bf16[512,2048]{1,0:T(8,128)(2,1)} fusion(bf16[1408,2048]{0,1:T(8,128)(2,1)} %all-gather.5.cloned.1.call-done, bf16[512,2048]{1,0:T(8,128)(2,1)} %bitcast.54, bf16[2048,2816]{1,0:T(8,128)(2,1)} %all-gather.3.cloned.1.call-done, f32[512,1408]{1,0:T(8,128)} %fusion.14), kind=kOutput, calls=%fused_computation.31 | convolution fusion | flops 5910953984 | bytes 18612224 | tf_op jit(solution)/shard_map/dot_general | solution.py:156
  195.4 29.0 %reduce-scatter.2.cloned.1.call-done = bf16[128,2048]{1,0:T(8,128)(2,1)} async-done(((bf16[512,2048]{1,0:T(8,128)(2,1)}), bf16[128,2048]{1,0:T(8,128)(2,1)}) %reduce-scatter.2.cloned.1.call-update) | async-done | bytes 524304 | tf_op jit(solution)/shard_map/reduce_scatter | solution.py:155
  224.4 2.2 add_convert_fusion
  (47 shorter events, 2.7 us)
Async XLA Ops:
  6.5 25.6 %copy-start = (bf16[512,2048]{1,0:T(8,128)(2,1)S(1)}, bf16[512,2048]{1,0:T(8,128)(2,1)}, u32[]{:S(2)}) copy-start(bf16[512,2048]{1,0:T(8,128)(2,1)} %param.18) | copy-start | bytes 6291460
  6.5 95.5 %all-gather.3.cloned.1.call-start = ((), (), s32[]{:S(2)}) async-start(), calls=%async_computation.3 | async-start | bytes 11714560 | tf_op jit(solution)/shard_map/all_gather | solution.py:64
  8.3 173.2 %all-gather.5.cloned.1.call-start = ((), (), s32[]{:S(2)}) async-start(), calls=%async_computation.4 | async-start | bytes 5857280 | tf_op jit(solution)/shard_map/all_gather | solution.py:99
  9.9 6.5 %collective-permute-start = (bf16[2,128,128]{2,1,0:T(8,128)(2,1)S(1)}, bf16[2,128,128]{2,1,0:T(8,128)(2,1)S(1)}, u32[]{:S(2)}, u32[]{:S(2)}) collective-permute-start(bf16[2,128,128]{2,1,0:T(8,128)(2,1)S(1)} %get-tuple-element.122), channel_id=1, source_target_pairs={{0,4},{4,8},{8,12},{12,16},{16,20},{20,24},{24,28},{28,32},{32,36}... | collective-permute-start | bytes 196616 | tf_op jit(solution)/shard_map/ppermute | solution.py:20
  14.4 5.6 %collective-permute-start.1 = (bf16[2,128,128]{2,1,0:T(8,128)(2,1)S(1)}, bf16[2,128,128]{2,1,0:T(8,128)(2,1)S(1)}, u32[]{:S(2)}, u32[]{:S(2)}) collective-permute-start(bf16[2,128,128]{2,1,0:T(8,128)(2,1)S(1)} %get-tuple-element.123), channel_id=1, source_target_pairs={{4,0},{8,4},{12,8},{16,12},{20,16},{24,20},{28,24},{32,28},{36,32}... | collective-permute-start | bytes 196616 | tf_op jit(solution)/shard_map/ppermute | solution.py:22
  23.6 0.7 copy-start.2
  24.7 1.0 copy-start.4
  25.8 0.8 copy-start.5
  29.1 0.7 copy-start.2
  30.2 1.0 copy-start.4
  31.3 0.8 copy-start.5
  35.7 29.2 %all-to-all-start = ((bf16[4,128,2048]{2,1,0:T(8,128)(2,1)}), bf16[4,128,2048]{2,1,0:T(8,128)(2,1)}, u32[]{:S(2)}, u32[]{:S(2)}) async-start(bf16[4,128,2048]{2,1,0:T(8,128)(2,1)} %bitcast.52), calls=%async_computation | async-start | bytes 4194304 | tf_op jit(solution)/shard_map/all_to_all | solution.py:36
  40.2 184.2 %reduce-scatter.2.cloned.1.call-start = ((), (), s32[]{:S(2)}) async-start(), calls=%async_computation.5 | async-start | bytes 2621440 | tf_op jit(solution)/shard_map/reduce_scatter | solution.py:155
  40.2 27.2 %copy-start.3 = (f32[2048]{0:T(1024)S(1)}, f32[2048]{0:T(1024)}, u32[]{:S(2)}) copy-start(f32[2048]{0:T(1024)} %param.17) | copy-start | bytes 24580
  64.9 2.2 copy-start.1
Sparse Core Ops, SparseCore 0:
  10.1 91.8 all-gather.2
  104.7 76.7 all-gather.4
  195.5 28.8 reduce-scatter.1
where the time goes:
time: 234 us; the launch traced here: 233 us
  waiting for transfers between devices  133 us (57%)
  blocking collectives  30 us (13%)
  matrix products  27.7 us (12%)
  between operations  13.2 us (6%)
  starting transfers between devices  10.9 us (5%)
  other arithmetic  9.91 us (4%)
  local copies, waits for them, and re-layouts  6.4 us (3%)
    all_gather x1, waiting for transfers between devices, fetch_down(): return lax.all_gather(down_weight, 'sp', axis=1, tiled=True)  71.3 us
    all_to_all x1, blocking collectives, sent_to_all(): lax.all_to_all(jnp.broadcast_to(value[None], (size, *value.shape)), axis,...  30 us
    reduce_scatter x1, waiting for transfers between devices, shards(): lax.psum_scatter(jnp.dot(picked, down_whole, preferred_element_type=jnp.f...  29 us
    all_to_all x1, waiting for transfers between devices, sent_and_summed(): blocks = lax.all_to_all(split_up(value, dim, size), axis, 0, 0, tiled=True)  24.7 us
    dot_general x1, matrix products, shards(): jnp.dot(picked, down_whole, preferred_element_type=jnp.float32)  13.8 us
    dot_general x1, matrix products, shards(): jnp.dot(normed_all, gate_sectioned, preferred_element_type=jnp.float32)  8.23 us
  transfers between devices with their start and end apart: 6, of which 5 were waited for; matrix products, arithmetic and copies ran while one was open for 10% of the time, Pallas kernels for 0%

commit v1 on v0

--- a/solution.py
+++ b/solution.py
@@ -96,7 +96,7 @@
 
 
 def fetch_down(down_weight):
-    return lax.all_gather(down_weight, "sp", axis=1, tiled=True)
+    return jnp.concatenate(lax.all_gather(down_weight, "sp"), axis=1)
 
 
 def shards(

time: 234 us -> 242 us (1.034)
  blocking collectives: 30 us -> 0 us
  waiting for transfers between devices: 133 us -> 157 us
  local copies, waits for them, and re-layouts: 6.4 us -> 17.1 us
  starting transfers between devices: 10.9 us -> 15.6 us
    all_gather x1, waiting for transfers between devices: 4.12 us -> 77.8 us  [side_by_side(): lax.all_gather(both, axis, axis=dim, tiled=True)]
    all_gather x1, waiting for transfers between devices: 71.3 us -> 20.9 us  [fetch_down(): return jnp.concatenate(lax.all_gather(down_weight, 'sp'), axis=1)]
    all_to_all x1 -> x0, blocking collectives: 30 us -> none  [sent_to_all(): lax.all_to_all(jnp.broadcast_to(value[None], (size, *value.shape)), axis,...]
    reshape x0 -> x1, local copies, waits for them, and re-layouts: none -> 5.69 us  [fetch_down(): return jnp.concatenate(lax.all_gather(down_weight, 'sp'), axis=1)]
    all_to_all x0 -> x1, starting transfers between devices: none -> 4.45 us  [sent_to_all(): lax.all_to_all(jnp.broadcast_to(value[None], (size, *value.shape)), axis,...]
    unnamed x6 -> x7, local copies, waits for them, and re-layouts: 0.02 us -> 3.63 us
  transfers between devices with their start and end apart: 6 -> 7, of which waited for: 5 -> 5; matrix products, arithmetic and copies ran while one was open for 10% -> 12% of each run, Pallas kernels for 0% -> 0%
where the time goes in v1:
time: 242 us; the launch traced here: 241 us
  waiting for transfers between devices  157 us (65%)
  matrix products  27.7 us (11%)
  local copies, waits for them, and re-layouts  17.1 us (7%)
  starting transfers between devices  15.6 us (6%)
  between operations  13.2 us (5%)
  other arithmetic  9.77 us (4%)
    all_gather x1, waiting for transfers between devices, side_by_side(): lax.all_gather(both, axis, axis=dim, tiled=True)  77.8 us
    reduce_scatter x1, waiting for transfers between devices, shards(): lax.psum_scatter(jnp.dot(picked, down_whole, preferred_element_type=jnp.f...  28.8 us
    all_to_all x1, waiting for transfers between devices, sent_and_summed(): blocks = lax.all_to_all(split_up(value, dim, size), axis, 0, 0, tiled=True)  24.7 us
    all_gather x1, waiting for transfers between devices, fetch_down(): return jnp.concatenate(lax.all_gather(down_weight, 'sp'), axis=1)  20.9 us
    dot_general x1, matrix products, shards(): jnp.dot(picked, down_whole, preferred_element_type=jnp.float32)  13.8 us
    dot_general x1, matrix products, shards(): jnp.dot(normed_all, gate_sectioned, preferred_element_type=jnp.float32)  8.28 us
    reshape x1, local copies, waits for them, and re-layouts, fetch_down(): return jnp.concatenate(lax.all_gather(down_weight, 'sp'), axis=1)  5.69 us
  transfers between devices with their start and end apart: 7, of which 5 were waited for; matrix products, arithmetic and copies ran while one was open for 12% of the time, Pallas kernels for 0%

profile of v1, /device:TPU:1, one launch (start us, length us, event | category | flops | bytes accessed | tf_op | source)
XLA Modules:
  0.0 241.4 jit_solution(190697894647127214)
XLA Ops:
  6.5 0.7 all-gather.6.cloned.1.call-update
  7.3 1.6 pad_maximum_fusion.1
  9.0 0.8 pad_maximum_fusion.3
  9.8 4.5 %collective-permute-start = (bf16[2,128,128]{2,1,0:T(8,128)(2,1)S(1)}, bf16[2,128,128]{2,1,0:T(8,128)(2,1)S(1)}, u32[]{:S(2)}, u32[]{:S(2)}) collective-permute-start(bf16[2,128,128]{2,1,0:T(8,128)(2,1)S(1)} %get-tuple-element.129), channel_id=1, source_target_pairs={{0,4},{4,8},{8,12},{12,16},{16,20},{20,24},{24,28},{28,32},{32,36}... | collective-permute-start | bytes 196616 | tf_op jit(solution)/shard_map/ppermute | solution.py:20
  14.3 1.9 collective-permute-start.1
  16.2 3.6 %collective-permute-done.1 = bf16[2,128,128]{2,1,0:T(8,128)(2,1)S(1)} collective-permute-done((bf16[2,128,128]{2,1,0:T(8,128)(2,1)S(1)}, bf16[2,128,128]{2,1,0:T(8,128)(2,1)S(1)}, u32[]{:S(2)}, u32[]{:S(2)}) %collective-permute-start.1) | collective-permute-done | bytes 65568 | tf_op jit(solution)/shard_map/ppermute | solution.py:22
  19.9 1.0 pad_maximum_fusion
  20.9 11.1 %while.12 = (s32[]{:T(128)}, bf16[2,256,512]{2,1,0:T(8,128)(2,1)}, bf16[2,768,128]{2,1,0:T(8,128)(2,1)S(1)}, s32[2]{0:T(128)S(1)}, s32[]{:T(128)}, /*index=5*/bf...) while((s32[]{:T(128)}, bf16[2,256,512]{2,1,0:T(8,128)(2,1)}, ...), condition=%wide.region_3.4_spmd, body=%wide.region_0.3_spmd.sunk | while | flops 273420544 | bytes 14467520 | solution.py:133
  20.9 0.6 dynamic_slice.48
  22.5 1.0 constant_dynamic-slice_fusion.2
  23.6 0.5 fusion.47
  24.6 0.5 convolution_convert_fusion.4
  25.6 0.8 copy-done.5
  26.4 0.6 dynamic_slice.48
  28.0 1.0 constant_dynamic-slice_fusion.2
  29.2 0.5 fusion.47
  30.1 0.5 convolution_convert_fusion.4
  31.2 0.8 copy-done.5
  32.0 3.6 %convolution_convert_fusion.1 = bf16[512,2048]{1,0:T(8,128)(2,1)} fusion(bf16[512,512]{1,0:T(8,128)(2,1)} %bitcast.67, bf16[512,2048]{1,0:T(8,128)(2,1)S(1)} %copy-done), kind=kOutput, calls=%fused_computation.30 | convolution fusion | flops 1074790400 | bytes 4718592 | tf_op jit(solution)/shard_map/dot_general | solution.py:138
  35.6 4.4 %all-to-all-start = ((bf16[4,128,2048]{2,1,0:T(8,128)(2,1)}), bf16[4,128,2048]{2,1,0:T(8,128)(2,1)}, u32[]{:S(2)}, u32[]{:S(2)}) async-start(bf16[4,128,2048]{2,1,0:T(8,128)(2,1)} %bitcast.62), calls=%async_computation | async-start | bytes 4194304 | tf_op jit(solution)/shard_map/all_to_all | solution.py:36
  40.1 24.7 %all-to-all-done = bf16[4,128,2048]{2,1,0:T(8,128)(2,1)} async-done(((bf16[4,128,2048]{2,1,0:T(8,128)(2,1)}), bf16[4,128,2048]{2,1,0:T(8,128)(2,1)}, u32[]{:S(2)}, u32[]{:S(2)}) %all-to-all-start) | async-done | bytes 2097184 | tf_op jit(solution)/shard_map/all_to_all | solution.py:36
  64.8 2.2 convert_reduce_fusion
  67.5 1.6 broadcast_in_dim.44
  69.1 4.4 %all-to-all-start.1 = ((bf16[4,128,2048]{2,1,0:T(8,128)(2,1)}), bf16[4,128,2048]{2,1,0:T(8,128)(2,1)}, u32[]{:S(2)}, u32[]{:S(2)}) async-start(bf16[4,128,2048]{2,1,0:T(8,128)(2,1)} %broadcast_in_dim.44), calls=%async_computation.1 | async-start | bytes 4194304 | tf_op jit(solution)/shard_map/all_to_all | solution.py:42
  73.8 20.9 %all-gather.6.cloned.1.call-done = bf16[90112,32]{0,1:T(8,128)(2,1)} async-done(((bf16[1408,32]{0,1:T(8,128)(2,1)}), bf16[90112,32]{0,1:T(8,128)(2,1)}) %all-gather.6.cloned.1.call-update) | async-done | bytes 5767184 | tf_op jit(solution)/shard_map/all_gather | solution.py:99
  94.7 3.6 %copy.29 = bf16[4,8,64,1408]{3,2,1,0:T(8,128)(2,1)S(1)} copy(bf16[4,8,64,1408]{3,1,2,0:T(8,128)(2,1)} %bitcast.60) | data formatting | bytes 11534336
  98.3 5.7 %copy.23 = bf16[1408,64,32]{0,2,1:T(8,128)(2,1)} copy(bf16[1408,64,32]{0,1,2:T(8,128)(2,1)S(1)} %bitcast.58) | data formatting | bytes 11534336 | tf_op jit(solution)/shard_map/reshape | solution.py:99
  104.0 77.8 %all-gather.4.cloned.1.call-done = bf16[2048,2816]{1,0:T(8,128)(2,1)} async-done(((bf16[32,2816]{1,0:T(8,128)(2,1)}), bf16[2048,2816]{1,0:T(8,128)(2,1)}) %all-gather.4.cloned.1.call-update) | async-done | bytes 11534352 | tf_op jit(solution)/shard_map/all_gather | solution.py:64
  181.8 8.3 %fusion.14 = f32[512,1408]{1,0:T(8,128)} fusion(bf16[512,2048]{1,0:T(8,128)(2,1)} %bitcast.16, bf16[2048,2816]{1,0:T(8,128)(2,1)} %all-gather.4.cloned.1.call-done), kind=kOutput, calls=%fused_computation.25 | convolution fusion | flops 2952790016 | bytes 10747904 | tf_op jit(solution)/shard_map/dot_general | solution.py:150
  190.1 13.8 %convolution_convert_fusion.2 = bf16[512,2048]{1,0:T(8,128)(2,1)} fusion(bf16[1408,2048]{0,1:T(8,128)(2,1)} %bitcast.61, bf16[512,2048]{1,0:T(8,128)(2,1)} %bitcast.16, bf16[2048,2816]{1,0:T(8,128)(2,1)} %all-gather.4.cloned.1.call-done, f32[512,1408]{1,0:T(8,128)} %fusion.14), kind=kOutput, calls=%fused_computation.31 | convolution fusion | flops 5910953984 | bytes 18612224 | tf_op jit(solution)/shard_map/dot_general | solution.py:156
  203.9 28.8 %reduce-scatter.2.cloned.1.call-done = bf16[128,2048]{1,0:T(8,128)(2,1)} async-done(((bf16[512,2048]{1,0:T(8,128)(2,1)}), bf16[128,2048]{1,0:T(8,128)(2,1)}) %reduce-scatter.2.cloned.1.call-update) | async-done | bytes 524304 | tf_op jit(solution)/shard_map/reduce_scatter | solution.py:155
  232.7 2.2 add_convert_fusion
  (50 shorter events, 3.6 us)
Async XLA Ops:
  6.5 25.4 %copy-start = (bf16[512,2048]{1,0:T(8,128)(2,1)S(1)}, bf16[512,2048]{1,0:T(8,128)(2,1)}, u32[]{:S(2)}) copy-start(bf16[512,2048]{1,0:T(8,128)(2,1)} %param.18) | copy-start | bytes 6291460
  6.5 88.1 %all-gather.6.cloned.1.call-start = ((), (), s32[]{:S(2)}) async-start(), calls=%async_computation.5 | async-start | bytes 5857280 | tf_op jit(solution)/shard_map/all_gather | solution.py:99
  7.3 174.6 %all-gather.4.cloned.1.call-start = ((), (), s32[]{:S(2)}) async-start(), calls=%async_computation.3 | async-start | bytes 11714560 | tf_op jit(solution)/shard_map/all_gather | solution.py:64
  9.8 6.5 %collective-permute-start = (bf16[2,128,128]{2,1,0:T(8,128)(2,1)S(1)}, bf16[2,128,128]{2,1,0:T(8,128)(2,1)S(1)}, u32[]{:S(2)}, u32[]{:S(2)}) collective-permute-start(bf16[2,128,128]{2,1,0:T(8,128)(2,1)S(1)} %get-tuple-element.129), channel_id=1, source_target_pairs={{0,4},{4,8},{8,12},{12,16},{16,20},{20,24},{24,28},{28,32},{32,36}... | collective-permute-start | bytes 196616 | tf_op jit(solution)/shard_map/ppermute | solution.py:20
  14.3 5.6 %collective-permute-start.1 = (bf16[2,128,128]{2,1,0:T(8,128)(2,1)S(1)}, bf16[2,128,128]{2,1,0:T(8,128)(2,1)S(1)}, u32[]{:S(2)}, u32[]{:S(2)}) collective-permute-start(bf16[2,128,128]{2,1,0:T(8,128)(2,1)S(1)} %get-tuple-element.130), channel_id=1, source_target_pairs={{4,0},{8,4},{12,8},{16,12},{20,16},{24,20},{28,24},{32,28},{36,32}... | collective-permute-start | bytes 196616 | tf_op jit(solution)/shard_map/ppermute | solution.py:22
  23.4 0.7 copy-start.2
  24.6 1.0 copy-start.4
  25.6 0.8 copy-start.5
  29.0 0.7 copy-start.2
  30.1 1.0 copy-start.4
  31.2 0.8 copy-start.5
  35.6 29.2 %all-to-all-start = ((bf16[4,128,2048]{2,1,0:T(8,128)(2,1)}), bf16[4,128,2048]{2,1,0:T(8,128)(2,1)}, u32[]{:S(2)}, u32[]{:S(2)}) async-start(bf16[4,128,2048]{2,1,0:T(8,128)(2,1)} %bitcast.62), calls=%async_computation | async-start | bytes 4194304 | tf_op jit(solution)/shard_map/all_to_all | solution.py:36
  40.1 27.2 %copy-start.3 = (f32[2048]{0:T(1024)S(1)}, f32[2048]{0:T(1024)}, u32[]{:S(2)}) copy-start(f32[2048]{0:T(1024)} %param.17) | copy-start | bytes 24580
  64.8 2.2 copy-start.1
  69.1 34.9 %all-to-all-start.1 = ((bf16[4,128,2048]{2,1,0:T(8,128)(2,1)}), bf16[4,128,2048]{2,1,0:T(8,128)(2,1)}, u32[]{:S(2)}, u32[]{:S(2)}) async-start(bf16[4,128,2048]{2,1,0:T(8,128)(2,1)} %broadcast_in_dim.44), calls=%async_computation.1 | async-start | bytes 4194304 | tf_op jit(solution)/shard_map/all_to_all | solution.py:42
  73.6 159.1 %reduce-scatter.2.cloned.1.call-start = ((), (), s32[]{:S(2)}) async-start(), calls=%async_computation.4 | async-start | bytes 2621440 | tf_op jit(solution)/shard_map/reduce_scatter | solution.py:155
Sparse Core Ops, SparseCore 0:
  10.0 84.5 all-gather.5
  97.4 84.3 all-gather.3
  204.0 28.5 reduce-scatter.1
